TPU v7x, 32 devices: a whole 2x2x4 slice. The times are simulated.
32 devices in a mesh: ep: 8 (over z, x), tp: 4 (over y, core).
Axes of the slice: x: 2, y: 2, z: 4, core: 2. Of those that a mesh axis runs over, the one named last changes fastest.
Arguments:
- queries: bfloat16 [8192, 2048], P('ep', 'tp'), may hold values from -128 to 128
- key_heads: bfloat16 [8192, 1024], P('ep', 'tp'), may hold values from -6 to 6
- value_heads: bfloat16 [8192, 1024], P('ep', 'tp'), may hold values from -6 to 6
- sink_logits: float32 [32], P('tp'), may hold values from 1 to 5
- mix_weight: bfloat16 [2048, 2048], replicated, may hold values from -1 to 1
- expert_input: bfloat16 [4096, 2048], P(('ep', 'tp')), may hold values from -6 to 6
- norm_gain: float32 [2048], replicated, may hold values from 0.1 to 1.9
- routes: int32 [4096, 4], P(('ep', 'tp')), may hold values from 0 to 31, all different within a row; in each aligned block of 128 rows (0 to 127, 128 to 255, ...) at most 32 rows name the same one
- route_weights: float32 [4096, 4], P(('ep', 'tp')), may hold values from 0.1 to 1
- gate_weight: bfloat16 [32, 2048, 1024], P(('ep', 'tp')), may hold values from -0.375 to 0.375
- up_weight: bfloat16 [32, 2048, 1024], P(('ep', 'tp')), may hold values from -0.375 to 0.375
- down_weight: bfloat16 [32, 1024, 2048], P(('ep', 'tp')), may hold values from -0.046875 to 0.046875
Outputs:
- mixer_out: bfloat16 [8192, 2048], P(('ep', 'tp'))
- experts_out: bfloat16 [4096, 2048], P(('ep', 'tp'))
Inputs may be any that keep to these rules, and one draw needn't show every extreme that they name: `routes`: each row names 4 different experts; within the 128 rows of one device no expert is named more than 32 times, and in some devices' rows some expert is named exactly 32 times.
All inputs are finite; a program needn't handle non-finite values.
Results may differ from a plain program's by a relative error of at most 0.012.
The roundings to bfloat16 on the way count: a program that leaves them out, or rounds other values in their place, can miss the bound.
Values may be sent and summed in bfloat16 or wider, within the bound.
A program may use at most 128 MiB of HBM per device.

v0:
```python
import math

import jax
import jax.numpy as jnp
from jax import lax
from jax.sharding import PartitionSpec as P

HEAD_DIM = 64
WINDOW = 128
GRID_W = 64


ROPE_BASE = 10000.0
CLAMP_LIMIT = 7.0
GATE_SLOPE = 1.702
NORM_EPS = 1e-05


def with_halo(cells, sides, width):
    for axis, dim in sides:
        count = lax.axis_size(axis)
        ends = count - 1
        head = lax.slice_in_dim(cells, 0, width, axis=dim)
        tail = lax.slice_in_dim(cells, cells.shape[dim] - width, cells.shape[dim], axis=dim)
        cells = jnp.concatenate(
            [
                lax.ppermute(tail, axis, [(i, (i + 1) % count) for i in range(ends)]),
                cells,
                lax.ppermute(head, axis, [((i + 1) % count, i) for i in range(ends)]),
            ],
            axis=dim,
        )
    return cells


def rotate_pairs(table, grid_rows, grid_cols, head_width):
    length = table.shape[0]
    quarter = head_width // 4
    shaped = table.reshape(length, -1, 2, 2, quarter)
    freqs = ROPE_BASE ** (-jnp.arange(0, head_width // 2, 2, dtype=jnp.float32) / (head_width // 2))
    angles = jnp.stack([grid_rows, grid_cols], axis=-1)[:, :, None] * freqs
    cosines = jnp.cos(angles)[:, None]
    sine_part = jnp.sin(angles)[:, None]
    former = shaped[..., 0, :]
    latter = shaped[..., 1, :]
    turned = jnp.stack(
        [former * cosines - latter * sine_part, latter * cosines + former * sine_part], axis=-2
    )
    return turned.reshape(length, -1)


def grid_place(positions):
    return ((positions // GRID_W).astype(jnp.float32), (positions % GRID_W).astype(jnp.float32))


def normalize(tokens_in, gain_row):
    values = tokens_in.astype(jnp.float32)
    center = jnp.mean(values, axis=-1, keepdims=True)
    spread = jnp.mean(jnp.square(values - center), axis=-1, keepdims=True)
    return ((values - center) * lax.rsqrt(spread + NORM_EPS) * gain_row).astype(jnp.bfloat16)


def expert_rows(row_block, w_gate, w_lift, w_down):
    gate_pre = jnp.dot(row_block, w_gate, preferred_element_type=jnp.float32)
    lift_pre = jnp.dot(row_block, w_lift, preferred_element_type=jnp.float32)
    gate_pre = jnp.minimum(gate_pre, CLAMP_LIMIT)
    lift_pre = jnp.clip(lift_pre, -CLAMP_LIMIT, CLAMP_LIMIT)
    activated = ((lift_pre + 1.0) * gate_pre * jax.nn.sigmoid(GATE_SLOPE * gate_pre)).astype(
        jnp.bfloat16
    )
    return jnp.dot(activated, w_down, preferred_element_type=jnp.float32).astype(jnp.bfloat16)


def body(
    queries,
    key_heads,
    value_heads,
    sink_logits,
    mix_weight,
    expert_input,
    norm_gain,
    routes,
    route_weights,
    gate_weight,
    up_weight,
    down_weight,
):
    rows_here = queries.shape[0]
    global_length = rows_here * lax.axis_size("ep")
    heads_local = sink_logits.shape[0]
    kv_local = key_heads.shape[1] // HEAD_DIM
    group_size = heads_local // kv_local
    first_global = lax.axis_index("ep") * rows_here
    positions = first_global + jnp.arange(rows_here, dtype=jnp.int32)
    grid_rows, grid_cols = grid_place(positions)
    q_rot = rotate_pairs(queries.astype(jnp.float32), grid_rows, grid_cols, HEAD_DIM).astype(
        jnp.bfloat16
    )
    k_rot = rotate_pairs(key_heads.astype(jnp.float32), grid_rows, grid_cols, HEAD_DIM).astype(
        jnp.bfloat16
    )
    paired = jnp.stack([k_rot, value_heads])
    widened = with_halo(paired, (("ep", 1),), WINDOW)
    block_rows = math.gcd(rows_here, 512)
    key_span = block_rows + 2 * WINDOW
    sink_grid = sink_logits.reshape(kv_local, group_size)

    def one_block(block_index):
        first_row = block_index * block_rows
        q_blk = lax.dynamic_slice_in_dim(q_rot, first_row, block_rows, 0)
        q_blk = q_blk.reshape(block_rows, kv_local, group_size, HEAD_DIM)
        k_blk = lax.dynamic_slice_in_dim(widened[0], first_row, key_span, 0).reshape(
            key_span, kv_local, HEAD_DIM
        )
        v_blk = lax.dynamic_slice_in_dim(widened[1], first_row, key_span, 0).reshape(
            key_span, kv_local, HEAD_DIM
        )
        q_pos = first_global + first_row + jnp.arange(block_rows, dtype=jnp.int32)
        k_pos = first_global + first_row - WINDOW + jnp.arange(key_span, dtype=jnp.int32)
        inside = (
            (jnp.abs(q_pos[:, None] - k_pos[None, :]) <= WINDOW)
            & (k_pos >= 0)
            & (k_pos < global_length)
        )
        scores = jnp.einsum(
            "qkgd,skd->kgqs", q_blk, k_blk, preferred_element_type=jnp.float32
        ) * HEAD_DIM ** (-0.5)
        scores = jnp.where(inside, scores, -jnp.inf)
        peak = jnp.maximum(jnp.max(scores, axis=-1), sink_grid[:, :, None])
        weights_exp = jnp.exp(scores - peak[..., None])
        denominator = jnp.sum(weights_exp, axis=-1) + jnp.exp(sink_grid[:, :, None] - peak)
        chances = (weights_exp / denominator[..., None]).astype(jnp.bfloat16)
        blended = jnp.einsum("kgqs,skd->qkgd", chances, v_blk, preferred_element_type=jnp.float32)
        return blended.astype(jnp.bfloat16).reshape(block_rows, heads_local * HEAD_DIM)

    blocks = lax.map(one_block, jnp.arange(rows_here // block_rows, dtype=jnp.int32))
    attended = blocks.reshape(rows_here, heads_local * HEAD_DIM)
    token_rows = lax.all_to_all(attended, "tp", split_axis=0, concat_axis=1, tiled=True)
    mixer_out = jnp.dot(token_rows, mix_weight, preferred_element_type=jnp.float32).astype(
        jnp.bfloat16
    )
    experts = lax.axis_size("ep") * lax.axis_size("tp")
    tok_local, top_count = routes.shape
    capacity = 2 * tok_local * top_count // experts
    width = expert_input.shape[1]
    normed = normalize(expert_input, norm_gain)
    flat_routes = routes.reshape(-1)
    matches = (flat_routes[:, None] == jnp.arange(experts, dtype=jnp.int32)[None, :]).astype(
        jnp.int32
    )
    earlier = jnp.cumsum(matches, axis=0) - matches
    slots = jnp.sum(earlier * matches, axis=1)
    columns = flat_routes * capacity + slots
    token_of = jnp.arange(tok_local * top_count, dtype=jnp.int32) // top_count
    table = jnp.full((experts * capacity,), tok_local, jnp.int32).at[columns].set(token_of)
    padded_in = jnp.concatenate([normed, jnp.zeros((1, width), jnp.bfloat16)], axis=0)
    outgoing = jnp.take(padded_in, table, axis=0).reshape(experts, capacity, width)
    w_gate = gate_weight[0]
    w_lift = up_weight[0]
    w_down = down_weight[0]
    arrived = lax.all_to_all(outgoing, ("ep", "tp"), split_axis=0, concat_axis=0, tiled=True)
    sources, items, feature_count = arrived.shape
    produced = expert_rows(arrived.reshape(sources * items, feature_count), w_gate, w_lift, w_down)
    produced = produced.reshape(sources, items, feature_count)
    returned = lax.all_to_all(produced, ("ep", "tp"), split_axis=0, concat_axis=0, tiled=True)
    picked = jnp.take(returned.reshape(experts * capacity, width), columns, axis=0)
    picked = picked.reshape(tok_local, top_count, width)
    summed = jnp.sum(route_weights[..., None] * picked.astype(jnp.float32), axis=1)
    return (mixer_out, summed.astype(jnp.bfloat16))


def solution(mesh):
    return jax.shard_map(
        body,
        mesh=mesh,
        in_specs=(
            P("ep", "tp"),
            P("ep", "tp"),
            P("ep", "tp"),
            P("tp"),
            P(),
            P(("ep", "tp"), None),
            P(),
            P(("ep", "tp"), None),
            P(("ep", "tp"), None),
            P(("ep", "tp"), None, None),
            P(("ep", "tp"), None, None),
            P(("ep", "tp"), None, None),
        ),
        out_specs=(P(("ep", "tp"), None), P(("ep", "tp"), None)),
        check_vma=False,
    )
```

profile of v0, /device:TPU:7, one launch (start us, length us, event | category | flops | bytes accessed | tf_op | source)
XLA Modules:
  0.0 267.9 jit_solution(4954015058673358655)
XLA Ops:
  0.7 1.3 copy.34
  2.2 1.2 copy.35
  3.4 0.5 multiply_cosine_fusion
  4.2 0.7 pad_maximum_fusion.4
  4.9 3.2 %collective-permute-start = (bf16[2,128,256]{1,2,0:T(8,128)(2,1)}, bf16[2,128,256]{1,2,0:T(8,128)(2,1)S(1)}, u32[]{:S(2)}, u32[]{:S(2)}) collective-permute-start(bf16[2,128,256]{1,2,0:T(8,128)(2,1)} %get-tuple-element.118), channel_id=1, source_target_pairs={{0,4},{4,8},{8,12},{12,16},{16,20},{20,24},{24,28},{1,5},{5,9},{9,... | collective-permute-start | bytes 393224 | tf_op jit(solution)/shard_map/ppermute | solution.py:27
  8.1 2.1 collective-permute-start.1
  10.6 1.2 reduce-window.6
  11.8 0.2 slice_reduce_fusion
  12.4 2.4 scatter_custom_fusion
  15.0 0.3 fusion.23
  15.4 0.4 fusion.25
  15.9 6.0 %gather_fusion = bf16[1024,2048]{1,0:T(8,128)(2,1)} fusion(bf16[129,2048]{1,0:T(8,128)(2,1)S(1)} %concatenate.7, s32[1024]{0:T(1024)S(1)} %fusion.32), kind=kCustom, calls=%fused_computation | custom fusion | bytes 8392704 | tf_op jit(solution)/shard_map/jit(_take)/gather | solution.py:157
  21.9 4.6 %broadcast_select_fusion = bf16[32,32,2048]{2,1,0:T(8,128)(2,1)} fusion(bf16[32,32,2048]{2,1,0:T(8,128)(2,1)} %bitcast.106, pred[32,32]{1,0:T(8,128)(4,1)S(1)} %broadcast_in_dim.75), kind=kLoop, calls=%fused_computation.33 | loop fusion | flops 2097152 | bytes 8389632 | tf_op jit(solution)/shard_map/jit(_take)/select_n | solution.py:157
  26.4 7.6 %all-to-all-start.1 = ((bf16[32,32,2048]{2,1,0:T(8,128)(2,1)}), bf16[32,32,2048]{2,1,0:T(8,128)(2,1)}, u32[]{:S(2)}, u32[]{:S(2)}) async-start(bf16[32,32,2048]{2,1,0:T(8,128)(2,1)} %broadcast_select_fusion), calls=%async_computation.1 | async-start | bytes 8388608 | tf_op jit(solution)/shard_map/all_to_all | solution.py:161
  34.1 1.5 copy.36
  35.5 0.2 convert.19
  35.8 0.3 subtract_convert_fusion
  36.3 1.0 pad_maximum_fusion
  37.3 47.2 %while.12 = (s32[]{:T(128)}, bf16[2,512,512]{2,1,0:T(8,128)(2,1)}, bf16[2,1280,256]{1,2,0:T(8,128)(2,1)S(1)}, s32[2]{0:T(128)S(1)}, s32[]{:T(128)}, /*index=5*/b...) while((s32[]{:T(128)}, bf16[2,512,512]{2,1,0:T(8,128)(2,1)}, ...), condition=%wide.region_3.4_spmd, body=%wide.region_0.3_spmd.sunk | while | flops 845295104 | bytes 99006360 | solution.py:136
  37.4 0.6 dynamic_slice.27
  38.6 0.8 fusion.61
  39.5 0.8 constant_dynamic-slice_fusion.5
  40.4 6.6 %fusion.62 = (f32[4,2,512]{2,1,0:T(2,128)S(1)}, f32[4,768,512,2]{2,1,3,0:T(8,128)}) fusion(pred[512,768]{0,1:T(8,128)(4,1)S(1)} %fusion.61, bf16[768,4,64,1]{0,2,3,1:T(8,128)(2,1)S(1)} %bitcast.105, bf16[512,4,2,64]{0,3,2,1:T(8,128)(2,1)S(1)} %bitcast.104), kind=kOutput, calls=%fused_computation.7.clone.1 | convolution fusion | flops 412086272 | bytes 13910016 | tf_op jit(solution)/shard_map/while/body/eval_jaxpr/qkgd,skd->kgqs/dot_general | solution.py:125
  47.2 7.3 %fusion.63 = f32[4,2,512]{2,1,0:T(2,128)S(1)} fusion(f32[4,768,512,2]{2,1,3,0:T(8,128)} %get-tuple-element.181, f32[4,2,512]{2,1,0:T(2,128)S(1)} %broadcast_maximum_fusion.2, pred[512,768]{0,1:T(8,128)(4,1)S(1)} %fusion.61), kind=kLoop, calls=%fused_computation.6.clone.1 | loop fusion | flops 12578816 | bytes 13008896 | tf_op jit(solution)/shard_map/while/body/eval_jaxpr/reduce_sum | solution.py:131
  54.6 0.7 copy-done
  55.3 4.6 %fusion.64 = bf16[4,64,2,512]{3,1,2,0:T(8,128)(2,1)S(1)} fusion(bf16[768,4,64,1]{0,2,3,1:T(8,128)(2,1)} %bitcast.109, f32[4,768,512,2]{2,1,3,0:T(8,128)S(1)} %copy-done, f32[4,2,512]{2,1,0:T(2,128)S(1)} %exponential_add_fusion.2, f32[4,2,512]{2,1,0:T(2,128)S(1)} %broadcast_maximum_fusion.2, pred[512,768]{0,1:T(8,128)(4,1)S(1)} %fusion.61), kind=kOutput, calls=%fused_computation.12.clone.1 | convolution fusion | flops 418643968 | bytes 13926400 | tf_op jit(solution)/shard_map/while/body/eval_jaxpr/kgqs,skd->qkgd/dot_general | solution.py:133
  59.9 0.2 copy.55
  60.1 0.8 constant_dynamic-update-slice_fusion.2
  61.0 0.6 dynamic_slice.27
  62.2 0.8 fusion.61
  63.1 0.8 constant_dynamic-slice_fusion.5
  64.0 6.6 %fusion.62 = (f32[4,2,512]{2,1,0:T(2,128)S(1)}, f32[4,768,512,2]{2,1,3,0:T(8,128)}) fusion(pred[512,768]{0,1:T(8,128)(4,1)S(1)} %fusion.61, bf16[768,4,64,1]{0,2,3,1:T(8,128)(2,1)S(1)} %bitcast.105, bf16[512,4,2,64]{0,3,2,1:T(8,128)(2,1)S(1)} %bitcast.104), kind=kOutput, calls=%fused_computation.7.clone.1 | convolution fusion | flops 412086272 | bytes 13910016 | tf_op jit(solution)/shard_map/while/body/eval_jaxpr/qkgd,skd->kgqs/dot_general | solution.py:125
  70.8 7.3 %fusion.63 = f32[4,2,512]{2,1,0:T(2,128)S(1)} fusion(f32[4,768,512,2]{2,1,3,0:T(8,128)} %get-tuple-element.181, f32[4,2,512]{2,1,0:T(2,128)S(1)} %broadcast_maximum_fusion.2, pred[512,768]{0,1:T(8,128)(4,1)S(1)} %fusion.61), kind=kLoop, calls=%fused_computation.6.clone.1 | loop fusion | flops 12578816 | bytes 13008896 | tf_op jit(solution)/shard_map/while/body/eval_jaxpr/reduce_sum | solution.py:131
  78.2 0.7 copy-done
  78.9 4.6 %fusion.64 = bf16[4,64,2,512]{3,1,2,0:T(8,128)(2,1)S(1)} fusion(bf16[768,4,64,1]{0,2,3,1:T(8,128)(2,1)} %bitcast.109, f32[4,768,512,2]{2,1,3,0:T(8,128)S(1)} %copy-done, f32[4,2,512]{2,1,0:T(2,128)S(1)} %exponential_add_fusion.2, f32[4,2,512]{2,1,0:T(2,128)S(1)} %broadcast_maximum_fusion.2, pred[512,768]{0,1:T(8,128)(4,1)S(1)} %fusion.61), kind=kOutput, calls=%fused_computation.12.clone.1 | convolution fusion | flops 418643968 | bytes 13926400 | tf_op jit(solution)/shard_map/while/body/eval_jaxpr/kgqs,skd->qkgd/dot_general | solution.py:133
  83.7 0.8 constant_dynamic-update-slice_fusion.2
  84.6 42.5 %all-to-all-done.1 = bf16[32,32,2048]{2,1,0:T(8,128)(2,1)} async-done(((bf16[32,32,2048]{2,1,0:T(8,128)(2,1)}), bf16[32,32,2048]{2,1,0:T(8,128)(2,1)}, u32[]{:S(2)}, u32[]{:S(2)}) %all-to-all-start.1) | async-done | bytes 4194336 | tf_op jit(solution)/shard_map/all_to_all | solution.py:161
  127.1 4.8 %all-to-all-start = ((bf16[4,256,512]{2,1,0:T(8,128)(2,1)}), bf16[4,256,512]{2,1,0:T(8,128)(2,1)S(1)}, u32[]{:S(2)}, u32[]{:S(2)}) async-start(bf16[4,256,512]{2,1,0:T(8,128)(2,1)} %bitcast.119), calls=%async_computation | async-start | bytes 2097152 | tf_op jit(solution)/shard_map/all_to_all | solution.py:138
  131.9 7.6 %fusion.12 = f32[1024,1024]{1,0:T(8,128)S(1)} fusion(bf16[1024,2048]{1,0:T(8,128)(2,1)} %bitcast.25, bf16[1,2048,1024]{2,1,0:T(8,128)(2,1)} %param.23), kind=kOutput, calls=%fused_computation.27 | convolution fusion | flops 4294967296 | bytes 12582912 | tf_op jit(solution)/shard_map/dot_general | solution.py:64
  139.6 8.0 %multiply_convert_fusion = bf16[1024,1024]{1,0:T(8,128)(2,1)S(1)} fusion(f32[1024,1024]{1,0:T(8,128)S(1)} %fusion.12, bf16[1024,2048]{1,0:T(8,128)(2,1)} %bitcast.25, bf16[1,2048,1024]{2,1,0:T(8,128)(2,1)S(1)} %copy-done.11), kind=kOutput, calls=%fused_computation.32 | convolution fusion | flops 4305453056 | bytes 14680064 | tf_op jit(solution)/shard_map/dot_general | solution.py:65
  147.6 6.1 %fusion.16 = bf16[1024,2048]{1,0:T(8,128)(2,1)} fusion(bf16[1024,1024]{1,0:T(8,128)(2,1)S(1)} %multiply_convert_fusion, bf16[1,1024,2048]{2,1,0:T(8,128)(2,1)S(1)} %copy-done.12), kind=kOutput, calls=%fused_computation.34 | convolution fusion | flops 4297064448 | bytes 10485760 | tf_op jit(solution)/shard_map/dot_general | solution.py:71
  153.7 5.3 %all-to-all-start.2 = ((bf16[32,32,2048]{2,1,0:T(8,128)(2,1)}), bf16[32,32,2048]{2,1,0:T(8,128)(2,1)}, u32[]{:S(2)}, u32[]{:S(2)}) async-start(bf16[32,32,2048]{2,1,0:T(8,128)(2,1)} %bitcast.116), calls=%async_computation.2 | async-start | bytes 8388608 | tf_op jit(solution)/shard_map/all_to_all | solution.py:165
  159.6 0.5 copy.38
  160.1 6.7 %convolution_convert_fusion = bf16[256,2048]{1,0:T(8,128)(2,1)} fusion(bf16[256,2048]{0,1:T(8,128)(2,1)S(1)} %bitcast.110, bf16[2048,2048]{1,0:T(8,128)(2,1)} %param.18), kind=kOutput, calls=%fused_computation.35 | convolution fusion | flops 2148007936 | bytes 10485760 | tf_op jit(solution)/shard_map/dot_general | solution.py:139
  166.8 85.3 %all-to-all-done.2 = bf16[32,32,2048]{2,1,0:T(8,128)(2,1)} async-done(((bf16[32,32,2048]{2,1,0:T(8,128)(2,1)}), bf16[32,32,2048]{2,1,0:T(8,128)(2,1)}, u32[]{:S(2)}, u32[]{:S(2)}) %all-to-all-start.2) | async-done | bytes 4194336 | tf_op jit(solution)/shard_map/all_to_all | solution.py:165
  252.1 7.1 %gather_fusion.1 = bf16[512,2048]{1,0:T(8,128)(2,1)S(1)} fusion(bf16[1024,2048]{1,0:T(8,128)(2,1)} %bitcast.30, s32[1024]{0:T(1024)S(1)} %pad_clamp_fusion), kind=kCustom, calls=%fused_computation.1 | custom fusion | bytes 4196352 | tf_op jit(solution)/shard_map/jit(_take)/gather | solution.py:166
  259.3 2.2 gather.15
  261.5 6.4 %multiply_reduce_fusion = bf16[128,2048]{1,0:T(8,128)(2,1)} fusion(bf16[128,4,2048]{2,1,0:T(4,128)(2,1)} %gather.15, f32[128,4]{1,0:T(8,128)S(1)} %copy.39, pred[128,4]{1,0:T(8,128)(4,1)S(1)} %copy.44), kind=kLoop, calls=%fused_computation.31 | loop fusion | flops 3932160 | bytes 2624000 | tf_op jit(solution)/shard_map/reduce_sum | solution.py:168
  (80 shorter events, 3.0 us)
Async XLA Ops:
  0.6 9.6 %copy-start.4 = (s32[128,4]{0,1:T(4,128)S(1)}, s32[128,4]{0,1:T(4,128)}, u32[]{:S(2)}) copy-start(s32[128,4]{0,1:T(4,128)} %param.21) | copy-start | bytes 6148
  0.7 14.2 %copy-start.1 = (bf16[128,2048]{1,0:T(8,128)(2,1)S(1)}, bf16[128,2048]{1,0:T(8,128)(2,1)}, u32[]{:S(2)}) copy-start(bf16[128,2048]{1,0:T(8,128)(2,1)} %param.19) | copy-start | bytes 1572868
  2.0 13.4 %copy-start.7 = (f32[2048]{0:T(1024)S(1)}, f32[2048]{0:T(1024)}, u32[]{:S(2)}) copy-start(f32[2048]{0:T(1024)} %param.20) | copy-start | bytes 24580
  4.9 31.3 %collective-permute-start = (bf16[2,128,256]{1,2,0:T(8,128)(2,1)}, bf16[2,128,256]{1,2,0:T(8,128)(2,1)S(1)}, u32[]{:S(2)}, u32[]{:S(2)}) collective-permute-start(bf16[2,128,256]{1,2,0:T(8,128)(2,1)} %get-tuple-element.118), channel_id=1, source_target_pairs={{0,4},{4,8},{8,12},{12,16},{16,20},{20,24},{24,28},{1,5},{5,9},{9,... | collective-permute-start | bytes 393224 | tf_op jit(solution)/shard_map/ppermute | solution.py:27
  8.1 28.2 %collective-permute-start.1 = (bf16[2,128,256]{1,2,0:T(8,128)(2,1)}, bf16[2,128,256]{1,2,0:T(8,128)(2,1)}, u32[]{:S(2)}, u32[]{:S(2)}) collective-permute-start(bf16[2,128,256]{1,2,0:T(8,128)(2,1)} %get-tuple-element.119), channel_id=1, source_target_pairs={{4,0},{8,4},{12,8},{16,12},{20,16},{24,20},{28,24},{5,1},{9,5},{13... | collective-permute-start | bytes 393224 | tf_op jit(solution)/shard_map/ppermute | solution.py:29
  12.4 9.5 %copy-start.2 = (s32[512]{0:T(512)}, s32[512]{0:T(512)S(1)}, u32[]{:S(2)}) copy-start(s32[512]{0:T(512)S(1)} %fusion.28) | copy-start | bytes 6148
  12.4 3.0 %copy-start.8 = (s32[512,1]{0,1:T(1,128)}, s32[512,1]{0,1:T(1,128)S(1)}, u32[]{:S(2)}) copy-start(s32[512,1]{0,1:T(1,128)S(1)} %compare_select_fusion) | copy-start | bytes 6148
  26.4 100.7 %all-to-all-start.1 = ((bf16[32,32,2048]{2,1,0:T(8,128)(2,1)}), bf16[32,32,2048]{2,1,0:T(8,128)(2,1)}, u32[]{:S(2)}, u32[]{:S(2)}) async-start(bf16[32,32,2048]{2,1,0:T(8,128)(2,1)} %broadcast_select_fusion), calls=%async_computation.1 | async-start | bytes 8388608 | tf_op jit(solution)/shard_map/all_to_all | solution.py:161
  35.8 1.5 copy-start.6
  47.2 8.2 %copy-start = (f32[4,768,512,2]{2,1,3,0:T(8,128)S(1)}, f32[4,768,512,2]{2,1,3,0:T(8,128)}, u32[]{:S(2)}) copy-start(f32[4,768,512,2]{2,1,3,0:T(8,128)} %get-tuple-element.181) | copy-start | bytes 37748740 | tf_op jit(solution)/shard_map/while
  70.8 8.2 %copy-start = (f32[4,768,512,2]{2,1,3,0:T(8,128)S(1)}, f32[4,768,512,2]{2,1,3,0:T(8,128)}, u32[]{:S(2)}) copy-start(f32[4,768,512,2]{2,1,3,0:T(8,128)} %get-tuple-element.181) | copy-start | bytes 37748740 | tf_op jit(solution)/shard_map/while
  127.1 26.6 %all-to-all-start = ((bf16[4,256,512]{2,1,0:T(8,128)(2,1)}), bf16[4,256,512]{2,1,0:T(8,128)(2,1)S(1)}, u32[]{:S(2)}, u32[]{:S(2)}) async-start(bf16[4,256,512]{2,1,0:T(8,128)(2,1)} %bitcast.119), calls=%async_computation | async-start | bytes 2097152 | tf_op jit(solution)/shard_map/all_to_all | solution.py:138
  131.9 7.7 %copy-start.11 = (bf16[1,2048,1024]{2,1,0:T(8,128)(2,1)S(1)}, bf16[1,2048,1024]{2,1,0:T(8,128)(2,1)}, u32[]{:S(2)}) copy-start(bf16[1,2048,1024]{2,1,0:T(8,128)(2,1)} %param.24) | copy-start | bytes 12582916
  139.6 8.0 %copy-start.12 = (bf16[1,1024,2048]{2,1,0:T(8,128)(2,1)S(1)}, bf16[1,1024,2048]{2,1,0:T(8,128)(2,1)}, u32[]{:S(2)}) copy-start(bf16[1,1024,2048]{2,1,0:T(8,128)(2,1)} %param.25) | copy-start | bytes 12582916
  153.7 5.4 %copy-start.3 = (s32[512]{0:T(512)S(1)}, s32[512]{0:T(512)}, u32[]{:S(2)}) copy-start(s32[512]{0:T(512)} %copy-done.2) | copy-start | bytes 6148
  153.7 5.5 %copy-start.5 = (s32[128,4]{0,1:T(4,128)S(1)}, s32[128,4]{0,1:T(4,128)}, u32[]{:S(2)}) copy-start(s32[128,4]{0,1:T(4,128)} %param.21) | copy-start | bytes 6148
  153.7 5.7 %copy-start.10 = (f32[128,4]{0,1:T(4,128)S(1)}, f32[128,4]{0,1:T(4,128)}, u32[]{:S(2)}) copy-start(f32[128,4]{0,1:T(4,128)} %param.22) | copy-start | bytes 6148
  153.7 5.8 %copy-start.9 = (s32[512,1]{0,1:T(1,128)S(1)}, s32[512,1]{0,1:T(1,128)}, u32[]{:S(2)}) copy-start(s32[512,1]{0,1:T(1,128)} %copy-done.8) | copy-start | bytes 6148
  153.7 98.4 %all-to-all-start.2 = ((bf16[32,32,2048]{2,1,0:T(8,128)(2,1)}), bf16[32,32,2048]{2,1,0:T(8,128)(2,1)}, u32[]{:S(2)}, u32[]{:S(2)}) async-start(bf16[32,32,2048]{2,1,0:T(8,128)(2,1)} %bitcast.116), calls=%async_computation.2 | async-start | bytes 8388608 | tf_op jit(solution)/shard_map/all_to_all | solution.py:165
where the time goes:
time: 271 us; the launch traced here: 268 us
  waiting for transfers between devices  128 us (47%)
  matrix products  50.9 us (19%)
  other arithmetic  33.1 us (12%)
  local copies, waits for them, and re-layouts  30.5 us (11%)
  starting transfers between devices  23 us (8%)
    all_to_all x1, waiting for transfers between devices, body(): lax.all_to_all(produced, ('ep', 'tp'), split_axis=0, concat_axis=0, tiled...  85.3 us
    all_to_all x1, waiting for transfers between devices, body(): lax.all_to_all(outgoing, ('ep', 'tp'), split_axis=0, concat_axis=0, tiled...  42.5 us
    reduce_sum x2, other arithmetic, one_block(): jnp.sum(weights_exp, axis=-1) + jnp.exp(sink_grid[:, :, None] - peak)  14.7 us
    dot_general x2, matrix products, one_block(): jnp.einsum('qkgd,skd->kgqs', q_blk, k_blk, preferred_element_type=jnp.flo...  13.3 us
    gather x2, local copies, waits for them, and re-layouts, body(): jnp.take(returned.reshape(experts * capacity, width), columns, axis=0)  9.35 us
    dot_general x2, matrix products, one_block(): jnp.einsum('kgqs,skd->qkgd', chances, v_blk, preferred_element_type=jnp.f...  9.16 us
    dot_general x1, matrix products, expert_rows(): lift_pre = jnp.dot(row_block, w_lift, preferred_element_type=jnp.float32)  8.02 us
    dot_general x1, matrix products, expert_rows(): gate_pre = jnp.dot(row_block, w_gate, preferred_element_type=jnp.float32)  7.64 us
  transfers between devices with their start and end apart: 5, of which 2 were waited for; matrix products, arithmetic and copies ran while one was open for 35% of the time, Pallas kernels for 0%

commit v1 on v0

v1 whole, which is shorter than its diff:
```python
import functools
import math

import jax
import jax.numpy as jnp
from jax import lax
from jax.experimental import pallas as pl
from jax.experimental.pallas import tpu as pltpu
from jax.sharding import Mesh
from jax.sharding import PartitionSpec as P

HEAD_DIM = 64
WINDOW = 128
GRID_W = 64
ROPE_BASE = 10000.0
CLAMP_LIMIT = 7.0
GATE_SLOPE = 1.702
NORM_EPS = 1e-05

F32 = jnp.float32
BF16 = jnp.bfloat16


def angle_tables(first, rows):
    half = HEAD_DIM // 2
    quarter = HEAD_DIM // 4
    positions = first + jnp.arange(rows, dtype=jnp.int32)
    lane = jnp.arange(2 * HEAD_DIM, dtype=jnp.int32) % HEAD_DIM
    freqs = ROPE_BASE ** (-jnp.arange(0, half, 2, dtype=F32) / half)
    lane_freq = jnp.tile(freqs, 2 * HEAD_DIM // quarter)
    by_row = (positions // GRID_W).astype(F32)[:, None]
    by_col = (positions % GRID_W).astype(F32)[:, None]
    angle = jnp.where((lane < half)[None, :], by_row, by_col) * lane_freq[None, :]
    sign = jnp.where(lane % half < quarter, -1.0, 1.0).astype(F32)
    return jnp.cos(angle), jnp.sin(angle) * sign[None, :]


def turn(cells, cosines, sines):
    quarter = HEAD_DIM // 4
    width = cells.shape[1]
    lane = lax.broadcasted_iota(jnp.int32, cells.shape, 1)
    ahead = pltpu.roll(cells, width - quarter, 1)
    behind = pltpu.roll(cells, quarter, 1)
    partner = jnp.where(lane % (2 * quarter) < quarter, ahead, behind)
    return cells * cosines + partner * sines


def attention_kernel(
    length, info, sink, q_ref, k_ref, v_ref, left_ref, right_ref, cos_ref, sin_ref, out_ref, k_scr, v_scr
):
    block = pl.program_id(0)
    rows_here = k_ref.shape[0]
    kv_local = k_scr.shape[0]
    bq = q_ref.shape[0]
    span = bq + 2 * WINDOW

    @pl.when(block == 0)
    def _():
        def place(source, values, start, count):
            for pair in range(kv_local // 2):
                cols = slice(pair * 128, pair * 128 + 128)
                turned = turn(
                    source[:, cols].astype(F32),
                    cos_ref[start : start + count, :],
                    sin_ref[start : start + count, :],
                ).astype(BF16)
                part = values[:, cols]
                for side in range(2):
                    k_scr[2 * pair + side, start : start + count, :] = turned[:, side * 64 : side * 64 + 64]
                    v_scr[2 * pair + side, start : start + count, :] = part[:, side * 64 : side * 64 + 64]

        place(left_ref[0], left_ref[1], 0, WINDOW)
        place(right_ref[0], right_ref[1], WINDOW + rows_here, WINDOW)
        for piece in range(rows_here // 256):
            at = piece * 256
            place(k_ref[at : at + 256, :], v_ref[at : at + 256, :], WINDOW + at, 256)

    first = pl.multiple_of(block * bq, bq)
    cosines = cos_ref[pl.ds(first + WINDOW, bq), :] * HEAD_DIM**-0.5
    sines = sin_ref[pl.ds(first + WINDOW, bq), :] * HEAD_DIM**-0.5
    row = lax.broadcasted_iota(jnp.int32, (2 * bq, span), 0) % bq
    col = lax.broadcasted_iota(jnp.int32, (2 * bq, span), 1)
    key_pos = info[0] + first - WINDOW + col
    inside = (col >= row) & (col <= row + 2 * WINDOW) & (key_pos >= 0) & (key_pos < length)
    top = lax.broadcasted_iota(jnp.int32, (2 * bq, 1), 0) < bq
    for g in range(kv_local):
        q = turn(q_ref[:, g * 128 : g * 128 + 128].astype(F32), cosines, sines).astype(BF16)
        q2 = jnp.concatenate([q[:, :64], q[:, 64:]], axis=0)
        k = k_scr[g, pl.ds(first, span), :]
        v = v_scr[g, pl.ds(first, span), :]
        scores = lax.dot_general(q2, k, (((1,), (1,)), ((), ())), preferred_element_type=F32)
        scores = jnp.where(inside, scores, -jnp.inf)
        logit = jnp.where(top, sink[2 * g], sink[2 * g + 1])
        peak = jnp.maximum(jnp.max(scores, axis=1, keepdims=True), logit)
        weights = jnp.exp(scores - peak)
        total = jnp.sum(weights, axis=1, keepdims=True) + jnp.exp(logit - peak)
        chances = (weights * (1.0 / total)).astype(BF16)
        blend = jnp.dot(chances, v, preferred_element_type=F32).astype(BF16)
        out_ref[:, g * 128 : g * 128 + 128] = jnp.concatenate([blend[:bq], blend[bq:]], axis=1)


def attention(queries, keys, values, left, right, cosines, sines, sink, first, length):
    rows, width = queries.shape
    kv_local = keys.shape[1] // HEAD_DIM
    bq = 128
    whole = pl.BlockSpec(memory_space=pltpu.VMEM)
    smem = pl.BlockSpec(memory_space=pltpu.SMEM)
    return pl.pallas_call(
        functools.partial(attention_kernel, length),
        grid=(rows // bq,),
        in_specs=[smem, smem, pl.BlockSpec((bq, width), lambda i: (i, 0))] + [whole] * 6,
        out_specs=pl.BlockSpec((bq, width), lambda i: (i, 0)),
        out_shape=jax.ShapeDtypeStruct((rows, width), BF16),
        scratch_shapes=[
            pltpu.VMEM((kv_local, rows + 2 * WINDOW, HEAD_DIM), BF16),
            pltpu.VMEM((kv_local, rows + 2 * WINDOW, HEAD_DIM), BF16),
        ],
        compiler_params=pltpu.CompilerParams(vmem_limit_bytes=32 * 1024 * 1024),
        cost_estimate=pl.CostEstimate(
            flops=rows * width * 384 * 4 * 8,
            bytes_accessed=rows * width * 8,
            transcendentals=rows * width * 6,
        ),
        name="attention",
    )(first, sink, queries, keys, values, left, right, cosines, sines)


def normalize(tokens_in, gain_row):
    values = tokens_in.astype(F32)
    center = jnp.mean(values, axis=-1, keepdims=True)
    spread = jnp.mean(jnp.square(values - center), axis=-1, keepdims=True)
    return ((values - center) * lax.rsqrt(spread + NORM_EPS) * gain_row).astype(BF16)


def ffn(row_block, w_gate, w_lift, w_down):
    gate_pre = jnp.dot(row_block, w_gate, preferred_element_type=F32)
    lift_pre = jnp.dot(row_block, w_lift, preferred_element_type=F32)
    gate_pre = jnp.minimum(gate_pre, CLAMP_LIMIT)
    lift_pre = jnp.clip(lift_pre, -CLAMP_LIMIT, CLAMP_LIMIT)
    activated = ((lift_pre + 1.0) * gate_pre * jax.nn.sigmoid(GATE_SLOPE * gate_pre)).astype(BF16)
    return jnp.dot(activated, w_down, preferred_element_type=F32).astype(BF16)


def body(
    queries,
    key_heads,
    value_heads,
    sink_logits,
    mix_weight,
    expert_input,
    norm_gain,
    routes,
    route_weights,
    gate_weight,
    up_weight,
    down_weight,
):
    n_z, n_x, n_tp = lax.axis_size("zz"), lax.axis_size("xx"), lax.axis_size("tp")
    n_ep = n_z * n_x
    experts = n_ep * n_tp
    plane = n_x * n_tp
    ep = lax.axis_index(("zz", "xx"))
    rows_here = queries.shape[0]
    tok, top_count = routes.shape
    capacity = 2 * tok * top_count // experts
    width = expert_input.shape[1]

    normed = normalize(expert_input, norm_gain)
    routing = jnp.concatenate([routes.astype(F32), route_weights], axis=1)
    routing = lax.all_gather(routing, "zz", axis=0)
    gathered = lax.all_gather(normed, "zz", axis=0)

    paired = jnp.stack([key_heads, value_heads])
    left = lax.ppermute(
        paired[:, rows_here - WINDOW :], ("zz", "xx"), [(i, i + 1) for i in range(n_ep - 1)]
    )
    right = lax.ppermute(paired[:, :WINDOW], ("zz", "xx"), [(i + 1, i) for i in range(n_ep - 1)])

    first_expert = lax.axis_index("zz") * plane
    named = routing[:, :, :top_count].astype(jnp.int32) - first_expert
    shares = routing[:, :, top_count:]
    here = named[:, :, :, None] == jnp.arange(plane, dtype=jnp.int32)
    member = jnp.any(here, axis=2)
    share = jnp.sum(jnp.where(here, shares[..., None], 0.0), axis=2)
    lower = jnp.tril(jnp.ones((tok, tok), BF16), -1)
    slot = jnp.einsum("ut,ztl->zul", lower, member.astype(BF16), preferred_element_type=F32)
    slot = jnp.where(member, slot.astype(jnp.int32), -1)
    chosen = slot[:, :, :, None] == jnp.arange(capacity, dtype=jnp.int32)
    pick = chosen.astype(BF16).reshape(n_z, tok, plane * capacity)
    outgoing = jnp.einsum("ztj,ztd->zjd", pick, gathered, preferred_element_type=F32).astype(BF16)
    outgoing = outgoing.reshape(n_z, plane, capacity, width).transpose(1, 0, 2, 3)
    arrived = lax.all_to_all(outgoing, ("xx", "tp"), split_axis=0, concat_axis=0, tiled=True)

    first = ep * rows_here
    cosines, sines = angle_tables(first - WINDOW, rows_here + 2 * WINDOW)
    attended = attention(
        queries,
        key_heads,
        value_heads,
        left,
        right,
        cosines,
        sines,
        sink_logits,
        first[None].astype(jnp.int32),
        rows_here * n_ep,
    )
    columns = attended.shape[1]
    token_rows = lax.all_to_all(
        attended.reshape(n_tp, rows_here // n_tp, columns), "tp", split_axis=0, concat_axis=0, tiled=True
    )

    produced = ffn(arrived.reshape(plane * n_z * capacity, width), gate_weight[0], up_weight[0], down_weight[0])
    produced = produced.reshape(plane, n_z, capacity, width)
    returned = lax.all_to_all(produced, ("xx", "tp"), split_axis=0, concat_axis=0, tiled=True)

    mixer_out = jnp.einsum(
        "trc,tcd->rd", token_rows, mix_weight.reshape(n_tp, columns, -1), preferred_element_type=F32
    ).astype(BF16)

    scaled = jnp.where(chosen, share[..., None], 0.0).reshape(n_z, tok, plane, capacity)
    coarse = scaled.astype(BF16)
    fine = (scaled - coarse.astype(F32)).astype(BF16)
    partial = jnp.einsum("ztls,lzsd->ztd", coarse, returned, preferred_element_type=F32)
    partial = partial + jnp.einsum("ztls,lzsd->ztd", fine, returned, preferred_element_type=F32)
    home = lax.all_to_all(partial.astype(BF16), "zz", split_axis=0, concat_axis=0, tiled=True)
    return mixer_out, jnp.sum(home.astype(F32), axis=0).astype(BF16)


def z_count(mesh, n_ep):
    coords = {getattr(d, "coords", (0, 0, 0))[2] for d in mesh.devices.flat}
    return len(coords) if n_ep % len(coords) == 0 else 1


def solution(mesh):
    n_ep, n_tp = mesh.shape["ep"], mesh.shape["tp"]
    n_z = z_count(mesh, n_ep)
    grid = Mesh(mesh.devices.reshape(n_z, n_ep // n_z, n_tp), ("zz", "xx", "tp"))
    ep = ("zz", "xx")
    every = ("zz", "xx", "tp")
    return jax.shard_map(
        body,
        mesh=grid,
        in_specs=(
            P(ep, "tp"),
            P(ep, "tp"),
            P(ep, "tp"),
            P("tp"),
            P(),
            P(every, None),
            P(),
            P(every, None),
            P(every, None),
            P(every, None, None),
            P(every, None, None),
            P(every, None, None),
        ),
        out_specs=(P(every, None), P(every, None)),
        check_vma=False,
    )
```

time: 271 us -> 287 us (1.059)
  blocking collectives: 0 us -> 61.9 us
  local copies, waits for them, and re-layouts: 30.5 us -> 0.78 us
  other arithmetic: 33.1 us -> 10.1 us
  Pallas kernels: 0 us -> 19 us
  matrix products: 50.9 us -> 33.4 us
  between operations: 1.07 us -> 14.2 us
  waiting for transfers between devices: 128 us -> 124 us
    all_to_all x3, waiting for transfers between devices: 128 us -> 46.2 us  [the longest x1 41 us: body(): lax.all_to_all(partial.astype(BF16), 'zz', split_axis=0, concat_axis=0, t...]
    all_to_all x0 -> x1, blocking collectives: none -> 51.4 us  [body(): lax.all_to_all(outgoing, ('xx', 'tp'), split_axis=0, concat_axis=0, tiled...]
    ppermute x2, waiting for transfers between devices: 0.01 us -> 43.6 us  [the longest x1 43.6 us: body(): lax.ppermute(paired[:, rows_here - WINDOW:], ('zz', 'xx'), [(i, i + 1) fo...]
    all_gather x0 -> x1, waiting for transfers between devices: none -> 34.5 us  [body(): gathered = lax.all_gather(normed, 'zz', axis=0)]
    reduce_sum x4 -> x2, other arithmetic: 21.2 us -> 1.32 us  [the longest x1 1.31 us: body(): return (mixer_out, jnp.sum(home.astype(F32), axis=0).astype(BF16))]
    pallas_call x0 -> x1, Pallas kernels: none -> 19 us  [attention(): pl.pallas_call(functools.partial(attention_kernel, length), grid=(rows //...]
    dot_general x8, matrix products: 50.9 us -> 33.4 us  [the longest x1 6.69 us: body(): jnp.einsum('trc,tcd->rd', token_rows, mix_weight.reshape(n_tp, columns, -...]
    gather x3 -> x0, local copies, waits for them, and re-layouts: 15.3 us -> none  [the longest x2 9.35 us: body(): jnp.take(returned.reshape(experts * capacity, width), columns, axis=0)]
  transfers between devices with their start and end apart: 5 -> 6, of which waited for: 2 -> 4; matrix products, arithmetic and copies ran while one was open for 35% -> 7% of each run, Pallas kernels for 0% -> 7%
where the time goes in v1:
time: 287 us; the launch traced here: 284 us
  waiting for transfers between devices  124 us (43%)
  blocking collectives  61.9 us (22%)
  matrix products  33.4 us (12%)
  starting transfers between devices  20.3 us (7%)
  Pallas kernels  19 us (7%)
  between operations  14.2 us (5%)
  other arithmetic  10.1 us (4%)
    all_to_all x1, blocking collectives, body(): lax.all_to_all(outgoing, ('xx', 'tp'), split_axis=0, concat_axis=0, tiled...  51.4 us
    ppermute x1, waiting for transfers between devices, body(): lax.ppermute(paired[:, rows_here - WINDOW:], ('zz', 'xx'), [(i, i + 1) fo...  43.6 us
    all_to_all x1, waiting for transfers between devices, body(): lax.all_to_all(partial.astype(BF16), 'zz', split_axis=0, concat_axis=0, t...  41 us
    all_gather x1, waiting for transfers between devices, body(): gathered = lax.all_gather(normed, 'zz', axis=0)  34.5 us
    pallas_call x1, Pallas kernels, attention(): pl.pallas_call(functools.partial(attention_kernel, length), grid=(rows //...  19 us
    all_gather x1, blocking collectives, body(): routing = lax.all_gather(routing, 'zz', axis=0)  10.5 us
    all_to_all x1, starting transfers between devices, body(): lax.all_to_all(produced, ('xx', 'tp'), split_axis=0, concat_axis=0, tiled...  6.72 us
    dot_general x1, matrix products, body(): jnp.einsum('trc,tcd->rd', token_rows, mix_weight.reshape(n_tp, columns, -...  6.69 us
  transfers between devices with their start and end apart: 6, of which 4 were waited for; matrix products, arithmetic and copies ran while one was open for 7% of the time, Pallas kernels for 7%

profile of v1, /device:TPU:7, one launch (start us, length us, event | category | flops | bytes accessed | tf_op | source)
XLA Modules:
  0.0 284.0 jit_solution(6733045938649177228)
XLA Ops:
  7.2 0.0 all-gather.4.cloned.1.call-start
  7.2 1.2 convert_reduce_fusion
  8.4 1.3 fusion.23
  9.8 2.2 fusion.25
  12.0 0.0 all-gather.4.cloned.1.call-update
  12.0 0.7 convert_element_type.63
  12.7 0.1 eq.50
  12.8 0.7 pad_maximum_fusion.2
  13.5 10.5 %all-gather = f32[512,8]{0,1:T(8,128)S(1)} all-gather(f32[128,8]{0,1:T(8,128)S(1)} %pad_maximum_fusion.2), channel_id=2, replica_groups=mesh['zz'=4,'xx'=2,'tp'=4] {'zz'}, dimensions={0}, use_global_device_ids=true | all-gather | bytes 20480 | tf_op jit(solution)/shard_map/all_gather | solution.py:170
  24.0 0.2 fusion.22
  24.2 0.2 bitcast_compare_fusion
  24.4 34.5 %all-gather.4.cloned.1.call-done = bf16[512,2048]{1,0:T(8,128)(2,1)} async-done(((bf16[128,2048]{1,0:T(8,128)(2,1)}), bf16[512,2048]{1,0:T(8,128)(2,1)}) %all-gather.4.cloned.1.call-update) | async-done | bytes 2097168 | tf_op jit(solution)/shard_map/all_gather | solution.py:171
  58.9 2.8 convolution_convert_fusion
  61.7 0.6 copy.38
  62.3 0.0 copy-start.4
  62.3 51.4 %all_to_all.20 = bf16[8,4,32,2048]{3,2,1,0:T(8,128)(2,1)S(1)} all-to-all(bf16[8,4,32,2048]{3,2,1,0:T(8,128)(2,1)S(1)} %bitcast.58), channel_id=1, replica_groups=mesh['zz'=4,'xx'=2,'tp'=4] {'xx','tp'}, dimensions={0} | all-to-all | bytes 8388608 | tf_op jit(solution)/shard_map/all_to_all | solution.py:192
  113.7 0.0 copy-done.4
  113.7 0.0 copy-start.5
  113.7 4.5 %fusion.3 = f32[1024,1024]{1,0:T(8,128)S(1)} fusion(bf16[1024,2048]{1,0:T(8,128)(2,1)S(1)} %bitcast.60, bf16[1,2048,1024]{2,1,0:T(8,128)(2,1)S(1)} %copy-done.4), kind=kOutput, calls=%fused_computation.4 | convolution fusion | flops 4294967296 | bytes 12582912 | tf_op jit(solution)/shard_map/dot_general | solution.py:136
  118.2 0.0 copy-done.5
  118.2 0.0 copy-start.6
  118.2 5.7 %multiply_convert_fusion = bf16[1024,1024]{1,0:T(8,128)(2,1)S(1)} fusion(f32[1024,1024]{1,0:T(8,128)S(1)} %fusion.3, bf16[1024,2048]{1,0:T(8,128)(2,1)S(1)} %bitcast.61, bf16[1,2048,1024]{2,1,0:T(8,128)(2,1)S(1)} %copy-done.5), kind=kOutput, calls=%fused_computation.9 | convolution fusion | flops 4305453056 | bytes 14680064 | tf_op jit(solution)/shard_map/dot_general | solution.py:137
  123.9 0.0 copy-done.6
  123.9 6.1 %fusion.7 = bf16[1024,2048]{1,0:T(8,128)(2,1)} fusion(bf16[1024,1024]{1,0:T(8,128)(2,1)S(1)} %multiply_convert_fusion, bf16[1,1024,2048]{2,1,0:T(8,128)(2,1)S(1)} %copy-done.6), kind=kOutput, calls=%fused_computation.11 | convolution fusion | flops 4297064448 | bytes 10485760 | tf_op jit(solution)/shard_map/dot_general | solution.py:141
  130.0 0.0 copy-start
  130.0 0.0 copy-start.1
  130.0 0.0 copy-start.2
  130.0 6.7 %all-to-all-start.2 = ((bf16[8,4,32,2048]{3,2,1,0:T(8,128)(2,1)}), bf16[8,4,32,2048]{3,2,1,0:T(8,128)(2,1)}, u32[]{:S(2)}, u32[]{:S(2)}) async-start(bf16[8,4,32,2048]{3,2,1,0:T(8,128)(2,1)} %bitcast.59), calls=%async_computation.2 | async-start | bytes 8388608 | tf_op jit(solution)/shard_map/all_to_all | solution.py:215
  136.7 0.0 copy-done
  136.7 0.0 copy-done.1
  136.8 1.9 collective-permute-start
  138.7 3.5 %collective-permute-start.1 = (bf16[2,128,256]{2,1,0:T(8,128)(2,1)S(1)}, bf16[2,128,256]{2,1,0:T(8,128)(2,1)S(1)}, u32[]{:S(2)}, u32[]{:S(2)}) collective-permute-start(bf16[2,128,256]{2,1,0:T(8,128)(2,1)S(1)} %get-tuple-element.2), channel_id=1, source_target_pairs={{4,0},{8,4},{12,8},{16,12},{20,16},{24,20},{28,24},{5,1},{9,5},{13... | collective-permute-start | bytes 393224 | tf_op jit(solution)/shard_map/ppermute | solution.py:177
  142.3 0.1 mul.65
  142.4 2.4 sine_multiply_fusion
  144.8 43.6 %collective-permute-done.left_ref = bf16[2,128,256]{2,1,0:T(8,128)(2,1)S(1)} collective-permute-done((bf16[2,128,256]{2,1,0:T(8,128)(2,1)S(1)}, bf16[2,128,256]{2,1,0:T(8,128)(2,1)S(1)}, u32[]{:S(2)}, u32[]{:S(2)}) %collective-permute-start) | collective-permute-done | bytes 131104 | tf_op jit(solution)/shard_map/ppermute | solution.py:174
  188.5 0.0 collective-permute-done.1.right_ref
  188.5 0.0 copy-done.2
  188.5 0.0 copy-done.3
  188.5 19.0 %attention.1 = bf16[1024,512]{1,0:T(8,128)(2,1)} custom-call(s32[1]{0:T(128)} %bitcast.info, f32[8]{0:T(128)S(1)} %copy-done.3, bf16[1024,512]{1,0:T(8,128)(2,1)S(1)} %copy-done.2, bf16[1024,256]{1,0:T(8,128)(2,1)S(1)} %copy-done, bf16[1024,256]{1,0:T(8,128)(2,1)S(1)} %copy-done.1, bf16[2,128,256]{2,1,0:T(8,128)(2,1)S(1)} %collective-permute-done.left_ref, ...), custom_call_target="tpu_custom_call" | custom-call | flops 6442450944 | bytes 4194304 | tf_op jit(solution)/shard_map/attention/pallas_call | solution.py:108
  207.4 0.0 all-to-all-done.2
  207.4 4.5 %all-to-all-start = ((bf16[4,256,512]{2,1,0:T(8,128)(2,1)}), bf16[4,256,512]{2,1,0:T(8,128)(2,1)S(1)}, u32[]{:S(2)}, u32[]{:S(2)}) async-start(bf16[4,256,512]{2,1,0:T(8,128)(2,1)} %bitcast.3), calls=%async_computation | async-start | bytes 2097152 | tf_op jit(solution)/shard_map/all_to_all | solution.py:209
  211.9 3.0 %fusion.10 = f32[4,128,2048,1]{2,1,3,0:T(8,128)S(1)} fusion(bf16[8,4,32,2048]{3,2,1,0:T(8,128)(2,1)} %all-to-all-done.2, f32[4,128,8]{1,2,0:T(8,128)S(1)} %select_reduce_fusion, s32[4,128,8]{1,2,0:T(8,128)S(1)} %fusion.22), kind=kOutput, calls=%fused_computation.12 | convolution fusion | flops 537657344 | bytes 8421376 | tf_op jit(solution)/shard_map/ztls,lzsd->ztd/dot_general | solution.py:225
  214.9 4.5 %fusion = bf16[4,128,2048]{2,1,0:T(8,128)(2,1)} fusion(f32[4,128,2048,1]{2,1,3,0:T(8,128)S(1)} %fusion.10, bf16[8,4,32,2048]{3,2,1,0:T(8,128)(2,1)} %all-to-all-done.2, f32[4,128,8]{1,2,0:T(8,128)S(1)} %select_reduce_fusion, s32[4,128,8]{1,2,0:T(8,128)S(1)} %fusion.22), kind=kOutput, calls=%fused_computation.1 | convolution fusion | flops 539230208 | bytes 10518528 | tf_op jit(solution)/shard_map/ztls,lzsd->ztd/dot_general | solution.py:224
  219.3 5.2 %all-to-all-done = bf16[4,256,512]{2,1,0:T(8,128)(2,1)S(1)} async-done(((bf16[4,256,512]{2,1,0:T(8,128)(2,1)}), bf16[4,256,512]{2,1,0:T(8,128)(2,1)S(1)}, u32[]{:S(2)}, u32[]{:S(2)}) %all-to-all-start) | async-done | bytes 1048608 | tf_op jit(solution)/shard_map/all_to_all | solution.py:209
  224.5 3.6 %all-to-all-start.3 = ((bf16[4,128,2048]{2,1,0:T(8,128)(2,1)}), bf16[4,128,2048]{2,1,0:T(8,128)(2,1)S(1)}, u32[]{:S(2)}, u32[]{:S(2)}) async-start(bf16[4,128,2048]{2,1,0:T(8,128)(2,1)} %fusion), calls=%async_computation.3 | async-start | bytes 4194304 | tf_op jit(solution)/shard_map/all_to_all | solution.py:226
  228.1 6.7 %fusion.16 = bf16[256,2048]{1,0:T(8,128)(2,1)} fusion(bf16[4,256,512]{2,1,0:T(8,128)(2,1)S(1)} %all-to-all-done, bf16[4,512,2048]{2,1,0:T(8,128)(2,1)} %bitcast.65), kind=kOutput, calls=%fused_computation.17 | convolution fusion | flops 2148007936 | bytes 10485760 | tf_op jit(solution)/shard_map/trc,tcd->rd/dot_general | solution.py:217
  234.8 41.0 %all-to-all-done.3 = bf16[4,128,2048]{2,1,0:T(8,128)(2,1)S(1)} async-done(((bf16[4,128,2048]{2,1,0:T(8,128)(2,1)}), bf16[4,128,2048]{2,1,0:T(8,128)(2,1)S(1)}, u32[]{:S(2)}, u32[]{:S(2)}) %all-to-all-start.3) | async-done | bytes 2097184 | tf_op jit(solution)/shard_map/all_to_all | solution.py:226
  275.8 1.3 reduce_sum.42
  (15 shorter events, 0.1 us)
Async XLA Ops:
  7.2 51.7 %all-gather.4.cloned.1.call-start = ((), (), s32[]{:S(2)}) async-start(), calls=%async_computation.4 | async-start | bytes 2621440 | tf_op jit(solution)/shard_map/all_gather | solution.py:171
  62.3 51.4 %copy-start.4 = (bf16[1,2048,1024]{2,1,0:T(8,128)(2,1)S(1)}, bf16[1,2048,1024]{2,1,0:T(8,128)(2,1)}, u32[]{:S(2)}) copy-start(bf16[1,2048,1024]{2,1,0:T(8,128)(2,1)} %param.21) | copy-start | bytes 12582916
  113.7 4.5 %copy-start.5 = (bf16[1,2048,1024]{2,1,0:T(8,128)(2,1)S(1)}, bf16[1,2048,1024]{2,1,0:T(8,128)(2,1)}, u32[]{:S(2)}) copy-start(bf16[1,2048,1024]{2,1,0:T(8,128)(2,1)} %param.22) | copy-start | bytes 12582916
  118.2 5.7 %copy-start.6 = (bf16[1,1024,2048]{2,1,0:T(8,128)(2,1)S(1)}, bf16[1,1024,2048]{2,1,0:T(8,128)(2,1)}, u32[]{:S(2)}) copy-start(bf16[1,1024,2048]{2,1,0:T(8,128)(2,1)} %param.23) | copy-start | bytes 12582916
  130.0 6.7 %copy-start = (bf16[1024,256]{1,0:T(8,128)(2,1)S(1)}, bf16[1024,256]{1,0:T(8,128)(2,1)}, u32[]{:S(2)}) copy-start(bf16[1024,256]{1,0:T(8,128)(2,1)} %k_ref.1) | copy-start | bytes 1572868
  130.0 6.7 %copy-start.1 = (bf16[1024,256]{1,0:T(8,128)(2,1)S(1)}, bf16[1024,256]{1,0:T(8,128)(2,1)}, u32[]{:S(2)}) copy-start(bf16[1024,256]{1,0:T(8,128)(2,1)} %v_ref.1) | copy-start | bytes 1572868
  130.0 58.5 %copy-start.2 = (bf16[1024,512]{1,0:T(8,128)(2,1)S(1)}, bf16[1024,512]{1,0:T(8,128)(2,1)}, u32[]{:S(2)}) copy-start(bf16[1024,512]{1,0:T(8,128)(2,1)} %q_ref.1) | copy-start | bytes 3145732
  130.0 58.5 %copy-start.3 = (f32[8]{0:T(128)S(1)}, f32[8]{0:T(128)}, u32[]{:S(2)}) copy-start(f32[8]{0:T(128)} %sink.1) | copy-start | bytes 100
  130.0 77.4 %all-to-all-start.2 = ((bf16[8,4,32,2048]{3,2,1,0:T(8,128)(2,1)}), bf16[8,4,32,2048]{3,2,1,0:T(8,128)(2,1)}, u32[]{:S(2)}, u32[]{:S(2)}) async-start(bf16[8,4,32,2048]{3,2,1,0:T(8,128)(2,1)} %bitcast.59), calls=%async_computation.2 | async-start | bytes 8388608 | tf_op jit(solution)/shard_map/all_to_all | solution.py:215
  136.8 51.7 %collective-permute-start = (bf16[2,128,256]{2,1,0:T(8,128)(2,1)S(1)}, bf16[2,128,256]{2,1,0:T(8,128)(2,1)S(1)}, u32[]{:S(2)}, u32[]{:S(2)}) collective-permute-start(bf16[2,128,256]{2,1,0:T(8,128)(2,1)S(1)} %get-tuple-element.3), channel_id=1, source_target_pairs={{0,4},{4,8},{8,12},{12,16},{16,20},{20,24},{24,28},{1,5},{5,9},{9,... | collective-permute-start | bytes 393224 | tf_op jit(solution)/shard_map/ppermute | solution.py:174
  138.7 49.8 %collective-permute-start.1 = (bf16[2,128,256]{2,1,0:T(8,128)(2,1)S(1)}, bf16[2,128,256]{2,1,0:T(8,128)(2,1)S(1)}, u32[]{:S(2)}, u32[]{:S(2)}) collective-permute-start(bf16[2,128,256]{2,1,0:T(8,128)(2,1)S(1)} %get-tuple-element.2), channel_id=1, source_target_pairs={{4,0},{8,4},{12,8},{16,12},{20,16},{24,20},{28,24},{5,1},{9,5},{13... | collective-permute-start | bytes 393224 | tf_op jit(solution)/shard_map/ppermute | solution.py:177
  207.4 17.0 %all-to-all-start = ((bf16[4,256,512]{2,1,0:T(8,128)(2,1)}), bf16[4,256,512]{2,1,0:T(8,128)(2,1)S(1)}, u32[]{:S(2)}, u32[]{:S(2)}) async-start(bf16[4,256,512]{2,1,0:T(8,128)(2,1)} %bitcast.3), calls=%async_computation | async-start | bytes 2097152 | tf_op jit(solution)/shard_map/all_to_all | solution.py:209
  224.5 51.3 %all-to-all-start.3 = ((bf16[4,128,2048]{2,1,0:T(8,128)(2,1)}), bf16[4,128,2048]{2,1,0:T(8,128)(2,1)S(1)}, u32[]{:S(2)}, u32[]{:S(2)}) async-start(bf16[4,128,2048]{2,1,0:T(8,128)(2,1)} %fusion), calls=%async_computation.3 | async-start | bytes 4194304 | tf_op jit(solution)/shard_map/all_to_all | solution.py:226
Sparse Core Ops, SparseCore 0:
  12.1 46.7 all-gather.3

commit v2 on v1

v2 whole, which is shorter than its diff:
```python
import functools
import math

import jax
import jax.numpy as jnp
from jax import lax
from jax.experimental import pallas as pl
from jax.experimental.pallas import tpu as pltpu
from jax.sharding import Mesh
from jax.sharding import PartitionSpec as P

HEAD_DIM = 64
WINDOW = 128
GRID_W = 64
ROPE_BASE = 10000.0
CLAMP_LIMIT = 7.0
GATE_SLOPE = 1.702
NORM_EPS = 1e-05

F32 = jnp.float32
BF16 = jnp.bfloat16


def angle_tables(first, rows):
    half = HEAD_DIM // 2
    quarter = HEAD_DIM // 4
    positions = first + jnp.arange(rows, dtype=jnp.int32)
    lane = jnp.arange(2 * HEAD_DIM, dtype=jnp.int32) % HEAD_DIM
    freqs = ROPE_BASE ** (-jnp.arange(0, half, 2, dtype=F32) / half)
    lane_freq = jnp.tile(freqs, 2 * HEAD_DIM // quarter)
    by_row = (positions // GRID_W).astype(F32)[:, None]
    by_col = (positions % GRID_W).astype(F32)[:, None]
    angle = jnp.where((lane < half)[None, :], by_row, by_col) * lane_freq[None, :]
    sign = jnp.where(lane % half < quarter, -1.0, 1.0).astype(F32)
    return jnp.cos(angle), jnp.sin(angle) * sign[None, :]


def turn(cells, cosines, sines):
    quarter = HEAD_DIM // 4
    width = cells.shape[1]
    lane = lax.broadcasted_iota(jnp.int32, cells.shape, 1)
    ahead = pltpu.roll(cells, width - quarter, 1)
    behind = pltpu.roll(cells, quarter, 1)
    partner = jnp.where(lane % (2 * quarter) < quarter, ahead, behind)
    return cells * cosines + partner * sines

MESH = pl.DeviceIdType.MESH


def kernel(
    sizes,
    sink,
    route_ref,
    x_ref,
    gain_ref,
    q_ref,
    k_ref,
    v_ref,
    cos_ref,
    sin_ref,
    wg_hbm,
    wu_hbm,
    wd_hbm,
    mix_hbm,
    mixer_ref,
    expert_ref,
    k_scr,
    v_scr,
    halo,
    att,
    att_in,
    routing,
    normed,
    outgoing,
    arrived,
    produced,
    returned,
    shares,
    partial,
    home,
    wg,
    wu,
    wd,
    mix,
    act,
    z_send,
    z_recv,
    rt_send,
    rt_recv,
    out_send,
    out_recv,
    back_send,
    back_recv,
    home_send,
    home_recv,
    att_send,
    att_recv,
    halo_send,
    halo_recv,
    load_sem,
):
    n_z, n_x, n_tp, top_count, capacity = sizes
    n_ep = n_z * n_x
    plane = n_x * n_tp
    slots = plane * capacity
    z, x, t = lax.axis_index("zz"), lax.axis_index("xx"), lax.axis_index("tp")
    me = x * n_tp + t
    ep = z * n_x + x
    rows_here, width_q = q_ref.shape
    tok, width = x_ref.shape
    length = rows_here * n_ep
    kv_local = k_scr.shape[0]
    bq = WINDOW
    span = bq + 2 * WINDOW
    blocks = rows_here // bq
    chunk = rows_here // n_tp

    def z_dev(b):
        return (b, x, t)

    def plane_dev(p):
        return (z, lax.div(p, n_tp), lax.rem(p, n_tp))

    def ep_dev(e):
        return (lax.div(e, n_x), lax.rem(e, n_x), t)

    after, before = lax.rem(ep + 1, n_ep), lax.rem(ep + n_ep - 1, n_ep)

    loads = [
        pltpu.make_async_copy(wg_hbm.at[0], wg, load_sem.at[0]),
        pltpu.make_async_copy(wu_hbm.at[0], wu, load_sem.at[1]),
        pltpu.make_async_copy(wd_hbm.at[0], wd, load_sem.at[2]),
        pltpu.make_async_copy(mix_hbm, mix, load_sem.at[3]),
    ]
    for load in loads:
        load.start()

    barrier = pltpu.get_barrier_semaphore()

    def greet_z(o, _):
        pl.semaphore_signal(barrier, inc=1, device_id=z_dev(lax.rem(z + o, n_z)), device_id_type=MESH)
        return 0

    def greet_plane(p, _):
        pl.semaphore_signal(
            barrier, inc=1, device_id=plane_dev(lax.rem(me + p, plane)), device_id_type=MESH
        )
        return 0

    lax.fori_loop(1, n_z, greet_z, 0)
    lax.fori_loop(1, plane, greet_plane, 0)
    for e in (after, before):
        pl.semaphore_signal(barrier, inc=1, device_id=ep_dev(e), device_id_type=MESH)

    for part in range(tok // 32):
        rows = slice(part * 32, part * 32 + 32)
        values = x_ref[rows, :].astype(F32)
        center = jnp.mean(values, axis=1, keepdims=True)
        spread = jnp.mean(jnp.square(values - center), axis=1, keepdims=True)
        normed[z, rows, :] = (
            (values - center) * lax.rsqrt(spread + NORM_EPS) * gain_ref[...]
        ).astype(BF16)
    routing[z] = route_ref[...]
    pl.semaphore_wait(barrier, n_z - 1 + plane - 1 + 2)

    def rt_copy(o):
        return pltpu.make_async_remote_copy(
            src_ref=routing.at[z],
            dst_ref=routing.at[z],
            send_sem=rt_send.at[o],
            recv_sem=rt_recv.at[z],
            device_id=z_dev(lax.rem(z + o, n_z)),
            device_id_type=MESH,
        )

    def z_copy(o):
        return pltpu.make_async_remote_copy(
            src_ref=normed.at[z],
            dst_ref=normed.at[z],
            send_sem=z_send.at[o],
            recv_sem=z_recv.at[z],
            device_id=z_dev(lax.rem(z + o, n_z)),
            device_id_type=MESH,
        )

    def halo_copy(source, which, start, target):
        return pltpu.make_async_remote_copy(
            src_ref=source.at[pl.ds(start, WINDOW)],
            dst_ref=halo.at[which],
            send_sem=halo_send.at[which],
            recv_sem=halo_recv.at[which],
            device_id=ep_dev(target),
            device_id_type=MESH,
        )

    halos = [
        halo_copy(k_ref, 0, rows_here - WINDOW, after),
        halo_copy(v_ref, 1, rows_here - WINDOW, after),
        halo_copy(k_ref, 2, 0, before),
        halo_copy(v_ref, 3, 0, before),
    ]
    for o in range(1, n_z):
        rt_copy(o).start()
    for copy in halos:
        copy.start()
    for o in range(1, n_z):
        z_copy(o).start()

    def await_bytes(ref, sem):
        pltpu.make_async_copy(ref, ref, sem).wait()

    def source_of(o):
        return lax.rem(z + n_z - o, n_z)

    slot_row = lax.broadcasted_iota(jnp.int32, (slots, tok), 0)
    lane_expert = (z * plane + lax.div(slot_row, capacity)).astype(F32)
    place_in = lax.rem(slot_row, capacity).astype(F32)
    upper = (
        lax.broadcasted_iota(jnp.int32, (tok, tok), 0) < lax.broadcasted_iota(jnp.int32, (tok, tok), 1)
    ).astype(F32).astype(BF16)

    def dispatch(o):
        b = source_of(o)
        if o > 0:
            await_bytes(routing.at[b], rt_recv.at[b])
            await_bytes(normed.at[b], z_recv.at[b])
        route = routing[b]
        member = jnp.zeros((slots, tok), F32)
        share = jnp.zeros((slots, tok), F32)
        for k in range(top_count):
            hit = route[k : k + 1, :] == lane_expert
            member = jnp.where(hit, 1.0, member)
            share = jnp.where(hit, route[top_count + k : top_count + k + 1, :], share)
        rank = jnp.dot(member.astype(BF16), upper, preferred_element_type=F32)
        pick = jnp.where(rank == place_in, member, 0.0)
        scaled = (share * pick).T
        coarse = scaled.astype(BF16)
        shares[b, 0] = coarse
        shares[b, 1] = (scaled - coarse.astype(F32)).astype(BF16)
        pick = pick.astype(BF16)

        def tile(j, _):
            cols = pl.ds(pl.multiple_of(j * 256, 256), 256)
            outgoing[b, :, cols] = jnp.dot(
                pick, normed[b, :, cols], preferred_element_type=F32
            ).astype(BF16)
            return 0

        lax.fori_loop(0, width // 256, tile, 0)
        exchange(outgoing, arrived, out_send, out_recv, b)

    def exchange(source, target, send, recv, b):
        mine = pl.ds(pl.multiple_of(me * capacity, capacity), capacity)

        def one(p, _):
            to = lax.rem(me + p, plane)
            pltpu.make_async_remote_copy(
                src_ref=source.at[b, pl.ds(pl.multiple_of(to * capacity, capacity), capacity)],
                dst_ref=target.at[b, mine],
                send_sem=send.at[b],
                recv_sem=recv.at[b],
                device_id=plane_dev(to),
                device_id_type=MESH,
            ).start()
            return 0

        lax.fori_loop(1, plane, one, 0)
        pltpu.make_async_copy(source.at[b, mine], target.at[b, mine], recv.at[b]).start()

    def place(source, values, at, count):
        for pair in range(kv_local // 2):
            cols = slice(pair * 128, pair * 128 + 128)
            turned = turn(
                source[:, cols].astype(F32), cos_ref[pl.ds(at, count), :], sin_ref[pl.ds(at, count), :]
            ).astype(BF16)
            piece = values[:, cols]
            for side in range(2):
                lanes = slice(side * 64, side * 64 + 64)
                k_scr[2 * pair + side, pl.ds(at, count), :] = turned[:, lanes]
                v_scr[2 * pair + side, pl.ds(at, count), :] = piece[:, lanes]

    def place_own(i, _):
        at = pl.multiple_of(i * 128, 128)
        place(k_ref[pl.ds(at, 128), :], v_ref[pl.ds(at, 128), :], WINDOW + at, 128)
        return 0

    row = lax.rem(lax.broadcasted_iota(jnp.int32, (2 * bq, span), 0), bq)
    col = lax.broadcasted_iota(jnp.int32, (2 * bq, span), 1)
    top = lax.broadcasted_iota(jnp.int32, (2 * bq, 1), 0) < bq

    def attend(block, _):
        first = pl.multiple_of(block * bq, bq)
        cosines = cos_ref[pl.ds(first + WINDOW, bq), :] * HEAD_DIM**-0.5
        sines = sin_ref[pl.ds(first + WINDOW, bq), :] * HEAD_DIM**-0.5
        key_pos = ep * rows_here + first - WINDOW + col
        inside = (col >= row) & (col <= row + 2 * WINDOW) & (key_pos >= 0) & (key_pos < length)
        for g in range(kv_local):
            q = q_ref[pl.ds(first, bq), g * 128 : g * 128 + 128].astype(F32)
            q = turn(q, cosines, sines).astype(BF16)
            q2 = jnp.concatenate([q[:, :64], q[:, 64:]], axis=0)
            k = k_scr[g, pl.ds(first, span), :]
            v = v_scr[g, pl.ds(first, span), :]
            scores = lax.dot_general(q2, k, (((1,), (1,)), ((), ())), preferred_element_type=F32)
            scores = jnp.where(inside, scores, -jnp.inf)
            logit = jnp.where(top, sink[2 * g], sink[2 * g + 1])
            peak = jnp.maximum(jnp.max(scores, axis=1, keepdims=True), logit)
            weights = jnp.exp(scores - peak)
            total = jnp.sum(weights, axis=1, keepdims=True) + jnp.exp(logit - peak)
            chances = (weights * (1.0 / total)).astype(BF16)
            blend = jnp.dot(chances, v, preferred_element_type=F32).astype(BF16)
            att[pl.ds(first, bq), g * 128 : g * 128 + 128] = jnp.concatenate(
                [blend[:bq], blend[bq:]], axis=1
            )
        return 0

    def send_heads():
        def one(p, _):
            to = lax.rem(t + p, n_tp)
            pltpu.make_async_remote_copy(
                src_ref=att.at[pl.ds(pl.multiple_of(to * chunk, chunk), chunk)],
                dst_ref=att_in.at[t],
                send_sem=att_send,
                recv_sem=att_recv,
                device_id=(z, x, to),
                device_id_type=MESH,
            ).start()
            return 0

        lax.fori_loop(1, n_tp, one, 0)
        own = pl.ds(pl.multiple_of(t * chunk, chunk), chunk)
        pltpu.make_async_copy(att.at[own], att_in.at[t], att_recv).start()

    def experts(o):
        b = source_of(o)
        await_bytes(arrived.at[b], out_recv.at[b])
        hidden = wg.shape[1]

        def up(j, _):
            cols = pl.ds(pl.multiple_of(j * 256, 256), 256)
            rows = arrived[b]
            gate = jnp.dot(rows, wg[:, cols], preferred_element_type=F32)
            lift = jnp.dot(rows, wu[:, cols], preferred_element_type=F32)
            gate = jnp.minimum(gate, CLAMP_LIMIT)
            lift = jnp.clip(lift, -CLAMP_LIMIT, CLAMP_LIMIT)
            act[:, cols] = ((lift + 1.0) * gate * jax.nn.sigmoid(GATE_SLOPE * gate)).astype(BF16)
            return 0

        def down(j, _):
            cols = pl.ds(pl.multiple_of(j * 256, 256), 256)
            produced[b, :, cols] = jnp.dot(
                act[...], wd[:, cols], preferred_element_type=F32
            ).astype(BF16)
            return 0

        lax.fori_loop(0, hidden // 256, up, 0)
        lax.fori_loop(0, width // 256, down, 0)
        exchange(produced, returned, back_send, back_recv, b)

    def combine(o):
        b = source_of(o)
        await_bytes(returned.at[b], back_recv.at[b])

        def tile(j, _):
            cols = pl.ds(pl.multiple_of(j * 256, 256), 256)
            rows = returned[b, :, cols]
            total = jnp.dot(shares[b, 0], rows, preferred_element_type=F32)
            total = total + jnp.dot(shares[b, 1], rows, preferred_element_type=F32)
            partial[o, :, cols] = total.astype(BF16)
            return 0

        lax.fori_loop(0, width // 256, tile, 0)
        if o > 0:
            home_copy(o).start()

    def home_copy(o):
        return pltpu.make_async_remote_copy(
            src_ref=partial.at[o],
            dst_ref=home.at[o],
            send_sem=home_send.at[o],
            recv_sem=home_recv.at[o],
            device_id=z_dev(source_of(o)),
            device_id_type=MESH,
        )

    def mixer():
        await_bytes(att_in, att_recv)
        loads[3].wait()

        def tile(j, _):
            cols = pl.ds(pl.multiple_of(j * 256, 256), 256)
            total = jnp.zeros((chunk, 256), F32)
            for s in range(n_tp):
                total = total + jnp.dot(
                    att_in[s], mix[s * width_q : s * width_q + width_q, cols], preferred_element_type=F32
                )
            mixer_ref[:, cols] = total.astype(BF16)
            return 0

        lax.fori_loop(0, width // 256, tile, 0)

    dispatch(0)
    lax.fori_loop(0, rows_here // 128, place_own, 0)
    for copy in halos:
        copy.wait()
    place(halo[0], halo[1], 0, WINDOW)
    place(halo[2], halo[3], WINDOW + rows_here, WINDOW)
    share_of = blocks // n_z
    lax.fori_loop(0, 2 * share_of, attend, 0)
    for o in range(1, 2):
        dispatch(o)
    lax.fori_loop(2 * share_of, blocks, attend, 0)
    send_heads()
    for load in loads[:3]:
        load.wait()
    experts(0)
    for o in range(2, n_z):
        dispatch(o)
        experts(o - 1)
    combine(1)
    experts(n_z - 1)
    mixer()
    for o in range(2, n_z):
        combine(o)
    combine(0)

    for o in range(1, n_z):
        rt_copy(o).wait_send()
        z_copy(o).wait_send()
        home_copy(o).wait()
    for b in range(n_z):
        gone = pl.ds(0, (plane - 1) * capacity)
        await_bytes(outgoing.at[b, gone], out_send.at[b])
        await_bytes(produced.at[b, gone], back_send.at[b])
    await_bytes(att.at[pl.ds(0, (n_tp - 1) * chunk)], att_send)

    for part in range(tok // 32):
        rows = slice(part * 32, part * 32 + 32)
        total = partial[0, rows, :].astype(F32)
        for o in range(1, n_z):
            total = total + home[o, rows, :].astype(F32)
        expert_ref[rows, :] = total.astype(BF16)


def body(
    queries,
    key_heads,
    value_heads,
    sink_logits,
    mix_weight,
    expert_input,
    norm_gain,
    routes,
    route_weights,
    gate_weight,
    up_weight,
    down_weight,
):
    n_z, n_x, n_tp = lax.axis_size("zz"), lax.axis_size("xx"), lax.axis_size("tp")
    n_ep = n_z * n_x
    plane = n_x * n_tp
    rows_here, width_q = queries.shape
    kv_local = key_heads.shape[1] // HEAD_DIM
    tok, top_count = routes.shape
    capacity = 2 * tok * top_count // (n_ep * n_tp)
    slots = plane * capacity
    width = expert_input.shape[1]
    hidden = gate_weight.shape[2]
    first = lax.axis_index(("zz", "xx")) * rows_here
    cosines, sines = angle_tables(first - WINDOW, rows_here + 2 * WINDOW)
    routing = jnp.concatenate([routes.astype(F32), route_weights], axis=1).T
    vmem = pl.BlockSpec(memory_space=pltpu.VMEM)
    smem = pl.BlockSpec(memory_space=pltpu.SMEM)
    anywhere = pl.BlockSpec(memory_space=pl.ANY)
    reach = rows_here + 2 * WINDOW
    dma = pltpu.SemaphoreType.DMA
    return pl.pallas_call(
        functools.partial(kernel, (n_z, n_x, n_tp, top_count, capacity)),
        in_specs=[smem] + [vmem] * 8 + [anywhere] * 4,
        out_specs=[vmem, vmem],
        out_shape=[
            jax.ShapeDtypeStruct((rows_here // n_tp, width), BF16),
            jax.ShapeDtypeStruct((tok, width), BF16),
        ],
        scratch_shapes=[
            pltpu.VMEM((kv_local, reach, HEAD_DIM), BF16),
            pltpu.VMEM((kv_local, reach, HEAD_DIM), BF16),
            pltpu.VMEM((4, WINDOW, key_heads.shape[1]), BF16),
            pltpu.VMEM((rows_here, width_q), BF16),
            pltpu.VMEM((n_tp, rows_here // n_tp, width_q), BF16),
            pltpu.VMEM((n_z, 2 * top_count, tok), F32),
            pltpu.VMEM((n_z, tok, width), BF16),
            pltpu.VMEM((n_z, slots, width), BF16),
            pltpu.VMEM((n_z, slots, width), BF16),
            pltpu.VMEM((n_z, slots, width), BF16),
            pltpu.VMEM((n_z, slots, width), BF16),
            pltpu.VMEM((n_z, 2, tok, slots), BF16),
            pltpu.VMEM((n_z, tok, width), BF16),
            pltpu.VMEM((n_z, tok, width), BF16),
            pltpu.VMEM((width, hidden), BF16),
            pltpu.VMEM((width, hidden), BF16),
            pltpu.VMEM((hidden, width), BF16),
            pltpu.VMEM(mix_weight.shape, BF16),
            pltpu.VMEM((slots, hidden), BF16),
            dma((n_z,)),
            dma((n_z,)),
            dma((n_z,)),
            dma((n_z,)),
            dma((n_z,)),
            dma((n_z,)),
            dma((n_z,)),
            dma((n_z,)),
            dma((n_z,)),
            dma((n_z,)),
            dma,
            dma,
            dma((4,)),
            dma((4,)),
            dma((4,)),
        ],
        compiler_params=pltpu.CompilerParams(
            collective_id=0, has_side_effects=True, vmem_limit_bytes=67043328
        ),
        name="layer",
    )(
        sink_logits,
        routing,
        expert_input,
        norm_gain[None, :],
        queries,
        key_heads,
        value_heads,
        cosines,
        sines,
        gate_weight,
        up_weight,
        down_weight,
        mix_weight,
    )


def z_count(mesh, n_ep):
    coords = {getattr(d, "coords", (0, 0, 0))[2] for d in mesh.devices.flat}
    return len(coords) if n_ep % len(coords) == 0 else 1


def solution(mesh):
    n_ep, n_tp = mesh.shape["ep"], mesh.shape["tp"]
    n_z = z_count(mesh, n_ep)
    grid = Mesh(mesh.devices.reshape(n_z, n_ep // n_z, n_tp), ("zz", "xx", "tp"))
    ep = ("zz", "xx")
    every = ("zz", "xx", "tp")
    return jax.shard_map(
        body,
        mesh=grid,
        in_specs=(
            P(ep, "tp"),
            P(ep, "tp"),
            P(ep, "tp"),
            P("tp"),
            P(),
            P(every, None),
            P(),
            P(every, None),
            P(every, None),
            P(every, None, None),
            P(every, None, None),
            P(every, None, None),
        ),
        out_specs=(P(every, None), P(every, None)),
        check_vma=False,
    )
```

time: 287 us -> 158 us (0.55); the launches traced: 284 us -> 158 us
  Pallas kernels: 19 us -> 147 us
  waiting for transfers between devices: 124 us -> 0 us
  blocking collectives: 61.9 us -> 0 us
  matrix products: 33.4 us -> 0 us
  starting transfers between devices: 20.3 us -> 0 us
  between operations: 14.2 us -> 0.67 us
  other arithmetic: 10.1 us -> 5.79 us
  local copies, waits for them, and re-layouts: 0.78 us -> 4.27 us
    pallas_call x1, Pallas kernels: 19 us -> 147 us  [body(): pl.pallas_call(functools.partial(kernel, (n_z, n_x, n_tp, top_count, capa...]
    all_to_all x1 -> x0, blocking collectives: 51.4 us -> none  [body(): lax.all_to_all(outgoing, ('xx', 'tp'), split_axis=0, concat_axis=0, tiled...]
    all_to_all x3 -> x0, waiting for transfers between devices: 46.2 us -> none  [the longest x1 41 us: body(): lax.all_to_all(partial.astype(BF16), 'zz', split_axis=0, concat_axis=0, t...]
    ppermute x2 -> x0, waiting for transfers between devices: 43.6 us -> none  [the longest x1 43.6 us: body(): lax.ppermute(paired[:, rows_here - WINDOW:], ('zz', 'xx'), [(i, i + 1) fo...]
    all_gather x1 -> x0, waiting for transfers between devices: 34.5 us -> none  [body(): gathered = lax.all_gather(normed, 'zz', axis=0)]
    dot_general x8 -> x0, matrix products: 33.4 us -> none  [the longest x1 6.69 us: body(): jnp.einsum('trc,tcd->rd', token_rows, mix_weight.reshape(n_tp, columns, -...]
    all_to_all x3 -> x0, starting transfers between devices: 14.8 us -> none  [the longest x1 6.72 us: body(): lax.all_to_all(produced, ('xx', 'tp'), split_axis=0, concat_axis=0, tiled...]
    all_gather x1 -> x0, blocking collectives: 10.5 us -> none  [body(): routing = lax.all_gather(routing, 'zz', axis=0)]
  transfers between devices with their start and end apart: 6 -> 0, of which waited for: 4 -> 0; matrix products, arithmetic and copies ran while one was open for 7% -> 0% of each run, Pallas kernels for 7% -> 0%
where the time goes in v2:
time: 158 us
  Pallas kernels  147 us (93%)
  other arithmetic  5.79 us (4%)
  local copies, waits for them, and re-layouts  4.27 us (3%)
    pallas_call x1, Pallas kernels, body(): pl.pallas_call(functools.partial(kernel, (n_z, n_x, n_tp, top_count, capa...  147 us
    unnamed x2, local copies, waits for them, and re-layouts  4.18 us
    mul x1, other arithmetic, angle_tables(): return (jnp.cos(angle), jnp.sin(angle) * sign[None, :])  3.79 us

profile of v2, /device:TPU:7, one launch (start us, length us, event | category | flops | bytes accessed | tf_op | source)
XLA Modules:
  0.0 158.1 jit_solution(1850612998314882445)
XLA Ops:
  0.7 0.7 convert_element_type.17
  1.4 1.3 maximum_bitcast_fusion.route_ref
  2.6 0.1 mul.34
  2.7 3.8 %sine_multiply_fusion = (f32[1280,128]{1,0:T(8,128)}, f32[1280,128]{1,0:T(8,128)}) fusion(f32[128]{0:T(128)S(1)} %compare_select_fusion.2, f32[128]{0:T(128)S(1)} %mul.34, f32[1280]{0:T(1024)S(1)} %get-tuple-element.5, f32[1280]{0:T(1024)S(1)} %get-tuple-element.4, pred[128]{0:T(512)(128)(4,1)S(1)} %broadcast_compare_fusion), kind=kLoop, calls=%fused_computation | loop fusion | flops 491520 | bytes 1322112 | tf_op jit(solution)/shard_map/mul | solution.py:35
  6.5 147.4 %layer.1 = (bf16[256,2048]{1,0:T(8,128)(2,1)}, bf16[128,2048]{1,0:T(8,128)(2,1)}) custom-call(f32[8]{0:T(128)} %sink.1, f32[8,128]{1,0:T(8,128)} %maximum_bitcast_fusion.route_ref, bf16[128,2048]{1,0:T(8,128)(2,1)} %x_ref.1, f32[1,2048]{1,0:T(1,128)} %bitcast.3, bf16[1024,512]{1,0:T(8,128)(2,1)} %q_ref.1, bf16[1024,256]{1,0:T(8,128)(2,1)} %k_ref.1, ...), custom_call_target="tpu_custom_call" | custom-call | tf_op jit(solution)/shard_map/layer/pallas_call | solution.py:476
  153.9 2.3 %copy.16 = bf16[256,2048]{1,0:T(8,128)(2,1)} copy(bf16[256,2048]{1,0:T(8,128)(2,1)} %get-tuple-element.8) | data formatting | bytes 2097152
  156.2 1.9 %copy.17 = bf16[128,2048]{1,0:T(8,128)(2,1)} copy(bf16[128,2048]{1,0:T(8,128)(2,1)} %get-tuple-element.9) | data formatting | bytes 1048576
  (5 shorter events, 0.0 us)

commit v3 on v2

--- a/solution.py
+++ b/solution.py
@@ -24,13 +24,12 @@
 def angle_tables(first, rows):
     half = HEAD_DIM // 2
     quarter = HEAD_DIM // 4
-    positions = first + jnp.arange(rows, dtype=jnp.int32)
     lane = jnp.arange(2 * HEAD_DIM, dtype=jnp.int32) % HEAD_DIM
     freqs = ROPE_BASE ** (-jnp.arange(0, half, 2, dtype=F32) / half)
     lane_freq = jnp.tile(freqs, 2 * HEAD_DIM // quarter)
-    by_row = (positions // GRID_W).astype(F32)[:, None]
-    by_col = (positions % GRID_W).astype(F32)[:, None]
-    angle = jnp.where((lane < half)[None, :], by_row, by_col) * lane_freq[None, :]
+    by_row = (first // GRID_W + jnp.arange(rows // GRID_W, dtype=jnp.int32)).astype(F32)
+    by_col = (jnp.arange(WINDOW, dtype=jnp.int32) % GRID_W).astype(F32)
+    angle = jnp.concatenate([by_row, by_col])[:, None] * lane_freq[None, :]
     sign = jnp.where(lane % half < quarter, -1.0, 1.0).astype(F32)
     return jnp.cos(angle), jnp.sin(angle) * sign[None, :]
 
@@ -267,12 +266,21 @@
         lax.fori_loop(1, plane, one, 0)
         pltpu.make_async_copy(source.at[b, mine], target.at[b, mine], recv.at[b]).start()
 
+    grid_rows = cos_ref.shape[0] - WINDOW
+    of_row = lax.rem(lax.broadcasted_iota(jnp.int32, (WINDOW, 128), 1), HEAD_DIM) < HEAD_DIM // 2
+
+    def angles(ref, at):
+        start = lax.div(at, GRID_W)
+        parts = [
+            jnp.broadcast_to(ref[pl.ds(start + i, 1), :], (GRID_W, 128)) for i in range(WINDOW // GRID_W)
+        ]
+        return jnp.where(of_row, jnp.concatenate(parts, axis=0), ref[grid_rows:, :])
+
     def place(source, values, at, count):
+        cosines, sines = angles(cos_ref, at), angles(sin_ref, at)
         for pair in range(kv_local // 2):
             cols = slice(pair * 128, pair * 128 + 128)
-            turned = turn(
-                source[:, cols].astype(F32), cos_ref[pl.ds(at, count), :], sin_ref[pl.ds(at, count), :]
-            ).astype(BF16)
+            turned = turn(source[:, cols].astype(F32), cosines, sines).astype(BF16)
             piece = values[:, cols]
             for side in range(2):
                 lanes = slice(side * 64, side * 64 + 64)
@@ -290,8 +298,8 @@
 
     def attend(block, _):
         first = pl.multiple_of(block * bq, bq)
-        cosines = cos_ref[pl.ds(first + WINDOW, bq), :] * HEAD_DIM**-0.5
-        sines = sin_ref[pl.ds(first + WINDOW, bq), :] * HEAD_DIM**-0.5
+        cosines = angles(cos_ref, first + WINDOW) * HEAD_DIM**-0.5
+        sines = angles(sin_ref, first + WINDOW) * HEAD_DIM**-0.5
         key_pos = ep * rows_here + first - WINDOW + col
         inside = (col >= row) & (col <= row + 2 * WINDOW) & (key_pos >= 0) & (key_pos < length)
         for g in range(kv_local):
@@ -354,7 +362,9 @@
 
         lax.fori_loop(0, hidden // 256, up, 0)
         lax.fori_loop(0, width // 256, down, 0)
-        exchange(produced, returned, back_send, back_recv, b)
+
+    def send_back(o):
+        exchange(produced, returned, back_send, back_recv, source_of(o))
 
     def combine(o):
         b = source_of(o)
@@ -416,10 +426,14 @@
     for o in range(2, n_z):
         dispatch(o)
         experts(o - 1)
-    combine(1)
+        send_back(o - 1)
+    if n_z > 2:
+        combine(1)
+    mixer()
     experts(n_z - 1)
-    mixer()
-    for o in range(2, n_z):
+    send_back(n_z - 1)
+    send_back(0)
+    for o in range(2 if n_z > 2 else 1, n_z):
         combine(o)
     combine(0)
 

time: 158 us -> 149 us (0.943)
  the two profiles are of different devices: /device:TPU:7 before, /device:TPU:5 now
where the time goes in v3:
time: 149 us
  Pallas kernels  141 us (95%)
  local copies, waits for them, and re-layouts  4.27 us (3%)
  other arithmetic  3.09 us (2%)
    pallas_call x1, Pallas kernels, body(): pl.pallas_call(functools.partial(kernel, (n_z, n_x, n_tp, top_count, capa...  141 us
    unnamed x2, local copies, waits for them, and re-layouts  4.18 us

profile of v3, /device:TPU:5, one launch (start us, length us, event | category | flops | bytes accessed | tf_op | source)
XLA Modules:
  0.0 149.1 jit_solution(4671096117902113783)
XLA Ops:
  0.7 0.1 pad_maximum_fusion
  0.8 0.7 convert_element_type.9
  1.5 1.3 maximum_bitcast_fusion.route_ref
  2.7 0.1 mul.40
  2.8 1.0 fusion
  3.8 141.0 %layer.1 = (bf16[256,2048]{1,0:T(8,128)(2,1)}, bf16[128,2048]{1,0:T(8,128)(2,1)}) custom-call(f32[8]{0:T(128)} %sink.1, f32[8,128]{1,0:T(8,128)} %maximum_bitcast_fusion.route_ref, bf16[128,2048]{1,0:T(8,128)(2,1)} %x_ref.1, f32[1,2048]{1,0:T(1,128)} %bitcast.3, bf16[1024,512]{1,0:T(8,128)(2,1)} %q_ref.1, bf16[1024,256]{1,0:T(8,128)(2,1)} %k_ref.1, ...), custom_call_target="tpu_custom_call" | custom-call | tf_op jit(solution)/shard_map/layer/pallas_call | solution.py:490
  144.9 2.3 %copy.16 = bf16[256,2048]{1,0:T(8,128)(2,1)} copy(bf16[256,2048]{1,0:T(8,128)(2,1)} %get-tuple-element.6) | data formatting | bytes 2097152
  147.2 1.9 %copy.17 = bf16[128,2048]{1,0:T(8,128)(2,1)} copy(bf16[128,2048]{1,0:T(8,128)(2,1)} %get-tuple-element.7) | data formatting | bytes 1048576
  (5 shorter events, 0.0 us)
